TPU v7x, 32 devices: a whole 2x2x4 slice. The times are simulated.
32 devices in a mesh: ep: 16 (over z, y, x), tp: 2 (over core).
Axes of the slice: x: 2, y: 2, z: 4, core: 2. Of those that a mesh axis runs over, the one named last changes fastest.
Arguments:
- tokens: bfloat16 [16, 2048], P('ep'), may hold values from -6 to 6
- norm_gain: float32 [2048], replicated, may hold values from 0.1 to 1.9
- w_query: bfloat16 [2048, 512], P('ep', 'tp'), may hold values from -0.125 to 0.125
- w_key: bfloat16 [2048, 512], P('ep', 'tp'), may hold values from -0.125 to 0.125
- w_value: bfloat16 [2048, 1024], P('ep', 'tp'), may hold values from -0.125 to 0.125
- w_outgate: bfloat16 [2048, 1024], P('ep', 'tp'), may hold values from -0.125 to 0.125
- decay_in: bfloat16 [2048, 16], replicated, may hold values from -0.125 to 0.125
- decay_out: bfloat16 [16, 512], P(None, 'tp'), may hold values from -1.5 to 1.5
- decay_bias: float32 [512], P('tp'), may hold values from -40 to 4
- gla_state: float32 [16, 2, 256, 512], P('ep', 'tp'), may hold values from -6 to 6
- head_gain: float32 [512], replicated, may hold values from 0.1 to 1.9
- w_output: bfloat16 [1024, 2048], P(None, 'ep'), may hold values from -0.1875 to 0.1875
- moe_gain: float32 [2048], replicated, may hold values from 0.1 to 1.9
- expert_ids: int32 [16, 6], replicated, may hold values from 0 to 15, all different within a row; in each aligned block of 16 rows (0 to 15, 16 to 31, ...) at most 12 rows name the same one
- route_weight: float32 [16, 6], replicated, may hold values from 0.2 to 1
- expert_gate: bfloat16 [16, 2048, 512], P('ep', None, 'tp'), may hold values from -0.125 to 0.125
- expert_up: bfloat16 [16, 2048, 512], P('ep', None, 'tp'), may hold values from -0.125 to 0.125
- expert_down: bfloat16 [16, 512, 2048], P('ep', 'tp'), may hold values from -0.25 to 0.25
- shared_gate: bfloat16 [2048, 512], P(None, 'tp'), may hold values from -0.125 to 0.125
- shared_up: bfloat16 [2048, 512], P(None, 'tp'), may hold values from -0.125 to 0.125
- shared_down: bfloat16 [512, 2048], P('tp'), may hold values from -0.25 to 0.25
Outputs:
- result: bfloat16 [16, 2048], P(None, 'ep')
- new_state: float32 [16, 2, 256, 512], P('ep', 'tp')
Inputs may be any that keep to these rules, and one draw needn't show every extreme that they name: `expert_ids`: each row names 6 different experts. No expert is named by more than 12 rows in all, a bound that some block reaches.
All inputs are finite; a program needn't handle non-finite values.
Results may differ from a plain program's by a relative error of at most 0.018.
Values may be sent and summed in bfloat16 or wider, within the bound.
No kernel may reach another device: no remote copies, remote signals or barrier semaphores. Data moves between devices by JAX's collectives and lax.ppermute only.
A program may use at most 64 MiB of HBM per device.

v0:
```python
import jax
import jax.numpy as jnp
from jax import lax
from jax.sharding import PartitionSpec as P

DK = 256
DV = 512
EPSILON = 1e-06
DECAY_TEMPER = 16.0


def rms_scale(values):
    return lax.rsqrt(jnp.mean(values * values, axis=-1, keepdims=True) + EPSILON)


def slot_positions(expert_ids, expert_count):
    flat_ids = expert_ids.reshape(-1)
    onehot = (flat_ids[:, None] == jnp.arange(expert_count, dtype=jnp.int32)[None, :]).astype(
        jnp.int32
    )
    before = jnp.cumsum(onehot, axis=0) - onehot
    position = jnp.sum(before * onehot, axis=1)
    return (flat_ids, position)


def expert_block(rows, moe_gain, gate_weight, up_weight, down_weight):
    row_float = rows.astype(jnp.float32)
    normal_rows = (row_float * rms_scale(row_float) * moe_gain).astype(jnp.bfloat16)
    gate_values = jnp.einsum(
        "ecd,edf->ecf", normal_rows, gate_weight, preferred_element_type=jnp.float32
    )
    upward = jnp.einsum("ecd,edf->ecf", normal_rows, up_weight, preferred_element_type=jnp.float32)
    active = (jax.nn.silu(gate_values) * upward).astype(jnp.bfloat16)
    return jnp.einsum(
        "ecf,efd->ecd", active, down_weight, preferred_element_type=jnp.float32
    ).astype(jnp.bfloat16)


def per_device(
    tokens,
    norm_gain,
    w_query,
    w_key,
    w_value,
    w_outgate,
    decay_in,
    decay_out,
    decay_bias,
    gla_state,
    head_gain,
    w_output,
    moe_gain,
    expert_ids,
    route_weight,
    expert_gate,
    expert_up,
    expert_down,
    shared_gate,
    shared_up,
    shared_down,
):
    ep_size = lax.axis_size("ep")
    tp_size = lax.axis_size("tp")
    seq_dev = tokens.shape[0]
    top_count = expert_ids.shape[1]
    exp_dev = expert_gate.shape[0]
    experts = exp_dev * ep_size
    all_rows = seq_dev * ep_size
    capacity = 2 * seq_dev * top_count // exp_dev
    heads_local = w_query.shape[1] // DK
    tok_float = tokens.astype(jnp.float32)
    normed = (tok_float * rms_scale(tok_float) * norm_gain).astype(jnp.bfloat16)
    span_sizes = (w_query.shape[1], w_key.shape[1], w_value.shape[1], w_outgate.shape[1])
    raw_columns, normed_columns = (
        lax.all_to_all(tokens, "ep", split_axis=1, concat_axis=0, tiled=True),
        lax.all_to_all(normed, "ep", split_axis=1, concat_axis=0, tiled=True),
    )
    joined = lax.psum_scatter(
        jnp.concatenate(
            [
                jnp.dot(normed_columns, weight, preferred_element_type=jnp.float32)
                for weight in (w_query, w_key, w_value, w_outgate)
            ],
            axis=1,
        ),
        "ep",
        scatter_dimension=0,
        tiled=True,
    )
    column_edges = [
        0,
        span_sizes[0],
        span_sizes[0] + span_sizes[1],
        span_sizes[0] + span_sizes[1] + span_sizes[2],
        sum(span_sizes),
    ]
    projected = tuple(
        (joined[:, column_edges[number] : column_edges[number + 1]] for number in range(4))
    )
    query_rows, key_rows, value_rows, gate_rows = (
        part_sum.astype(jnp.bfloat16) for part_sum in projected
    )
    decay_low = jnp.dot(normed, decay_in, preferred_element_type=jnp.float32).astype(jnp.bfloat16)
    decay_pre = jnp.dot(decay_low, decay_out, preferred_element_type=jnp.float32) + decay_bias
    decay_rate = jnp.exp(jax.nn.log_sigmoid(decay_pre) / DECAY_TEMPER).reshape(
        seq_dev, heads_local, DK
    )
    query_heads = query_rows.astype(jnp.float32).reshape(seq_dev, heads_local, DK) * DK ** (-0.5)
    key_heads = key_rows.astype(jnp.float32).reshape(seq_dev, heads_local, DK)
    value_heads = value_rows.astype(jnp.float32).reshape(seq_dev, heads_local, DV)
    new_state = (
        decay_rate[..., None] * gla_state + key_heads[..., None] * value_heads[:, :, None, :]
    )
    read_out = jnp.einsum("shk,shkv->shv", query_heads, new_state, precision=lax.Precision.HIGHEST)
    gate_heads = gate_rows.astype(jnp.float32).reshape(seq_dev, heads_local, DV)
    mixed_heads = (read_out * rms_scale(read_out) * head_gain * jax.nn.silu(gate_heads)).astype(
        jnp.bfloat16
    )
    head_weights = w_output.reshape(tp_size, heads_local * DV, w_output.shape[1])
    shard_rows = lax.all_gather(mixed_heads, ("ep", "tp"), axis=0, tiled=True)
    owners = lax.iota(jnp.int32, shard_rows.shape[0])
    select = (owners[:, None] % tp_size == lax.iota(jnp.int32, tp_size)[None, :]).astype(
        jnp.bfloat16
    )
    chosen = jnp.einsum(
        "mt,tcd->mcd", select, head_weights, preferred_element_type=jnp.float32
    ).astype(jnp.bfloat16)
    spread = jnp.einsum("msc,mcd->msd", shard_rows, chosen, preferred_element_type=jnp.float32)
    attention = (
        spread.reshape(ep_size, tp_size, seq_dev, -1)
        .sum(axis=1)
        .reshape(all_rows, -1)
        .astype(jnp.bfloat16)
    )
    hidden = (raw_columns.astype(jnp.float32) + attention.astype(jnp.float32)).astype(jnp.bfloat16)
    flat_ids, position = slot_positions(expert_ids, experts)
    owner_rows = lax.iota(jnp.int32, all_rows * top_count) // top_count
    slot_table = (
        jnp.full((experts, capacity), all_rows, jnp.int32).at[flat_ids, position].set(owner_rows)
    )
    padded = jnp.concatenate([hidden, jnp.zeros((1, hidden.shape[1]), jnp.bfloat16)], axis=0)
    routed_rows, shared_rows = (
        lax.all_to_all(padded[slot_table], "ep", split_axis=0, concat_axis=2, tiled=True),
        lax.all_to_all(
            hidden.reshape(ep_size, seq_dev, hidden.shape[1]),
            "ep",
            split_axis=0,
            concat_axis=2,
            tiled=True,
        ),
    )
    routed_part = expert_block(routed_rows, moe_gain, expert_gate, expert_up, expert_down)
    shared_part = expert_block(
        shared_rows, moe_gain, shared_gate[None], shared_up[None], shared_down[None]
    )
    routed_sum, shared_sum = (
        lax.psum(routed_part, "tp").astype(jnp.float32),
        lax.psum(shared_part, "tp").astype(jnp.float32),
    )
    routed_out = routed_sum.astype(jnp.bfloat16)
    shared_out = shared_sum.astype(jnp.bfloat16)
    back_routed, back_shared = (
        lax.all_to_all(routed_out, "ep", split_axis=2, concat_axis=0, tiled=True),
        lax.all_to_all(shared_out, "ep", split_axis=2, concat_axis=0, tiled=True),
    )
    picked = back_routed.reshape(experts * capacity, -1)[flat_ids * capacity + position]
    weighted = picked.astype(jnp.float32).reshape(all_rows, top_count, -1) * route_weight[..., None]
    moe_columns = jnp.sum(weighted, axis=1) + back_shared.reshape(all_rows, -1).astype(jnp.float32)
    result = (hidden.astype(jnp.float32) + moe_columns).astype(jnp.bfloat16)
    return (result, new_state)


def solution(mesh):
    return jax.shard_map(
        per_device,
        mesh=mesh,
        in_specs=(
            P("ep", None),
            P(),
            P("ep", "tp"),
            P("ep", "tp"),
            P("ep", "tp"),
            P("ep", "tp"),
            P(),
            P(None, "tp"),
            P("tp"),
            P("ep", "tp", None, None),
            P(),
            P(None, "ep"),
            P(),
            P(),
            P(),
            P("ep", None, "tp"),
            P("ep", None, "tp"),
            P("ep", "tp", None),
            P(None, "tp"),
            P(None, "tp"),
            P("tp", None),
        ),
        out_specs=(P(None, "ep"), P("ep", "tp", None, None)),
        check_vma=False,
    )
```

profile of v0, /device:TPU:0, one launch (start us, length us, event | category | flops | bytes accessed | tf_op | source)
XLA Modules:
  0.0 244.8 jit_solution(1949194534503189319)
XLA Ops:
  0.6 0.0 copy-start
  0.6 0.0 copy-start.11
  0.7 1.4 multiply_reduce_fusion.2
  2.8 1.3 convert_bitcast_fusion.3
  4.1 8.3 %all-to-all-start.1 = ((bf16[1,16,128]{2,0,1:T(2,128)(2,1)}), bf16[1,16,128]{2,0,1:T(2,128)(2,1)S(1)}, u32[]{:S(2)}, u32[]{:S(2)}) async-start(bf16[1,16,128]{2,0,1:T(2,128)(2,1)} %convert_bitcast_fusion.3), calls=%async_computation.1 | async-start | bytes 16384 | tf_op jit(solution)/shard_map/all_to_all | solution.py:76
  12.5 0.8 copy.66
  13.3 0.1 eq.33
  13.4 0.1 reshape.455
  13.5 0.1 fusion.20
  13.5 0.0 copy-start.10
  13.6 0.1 reduce_window_sum.11
  13.7 0.2 select_reduce_fusion
  13.9 5.4 %scatter_fusion = s32[16,12]{1,0:T(8,128)S(1)} fusion(s32[16,12]{1,0:T(8,128)S(1)} %broadcast_in_dim.7, s32[96]{0:T(128)S(1)} %get-tuple-element.7, s32[96]{0:T(128)S(1)} %and_select_fusion), kind=kCustom, calls=%fused_computation.2 | custom fusion | bytes 1920 | tf_op jit(solution)/shard_map/scatter | solution.py:139
  19.3 0.1 reshape.472
  19.4 1.1 fusion.11
  20.5 0.7 fusion.51
  21.2 4.2 %convolution_convert_fusion = bf16[32,512,128]{2,0,1:T(8,128)(2,1)} fusion(bf16[2,512,128]{2,1,0:T(8,128)(2,1)} %bitcast.143, s32[32]{0:T(128)S(1)} %and_select_fusion.1), kind=kOutput, calls=%fused_computation.5 | convolution fusion | flops 10485824 | bytes 4456576 | tf_op jit(solution)/shard_map/mt,tcd->mcd/dot_general | solution.py:125
  25.5 0.6 dynamic-slice
  26.0 0.0 all-to-all-done.1
  26.1 6.9 %all-to-all-start = ((bf16[1,16,128]{2,0,1:T(2,128)(2,1)}), bf16[1,16,128]{2,0,1:T(2,128)(2,1)S(1)}, u32[]{:S(2)}, u32[]{:S(2)}) async-start(bf16[1,16,128]{2,0,1:T(2,128)(2,1)} %bitcast), calls=%async_computation | async-start | bytes 16384 | tf_op jit(solution)/shard_map/all_to_all | solution.py:75
  33.0 0.1 fusion.36
  33.1 0.1 fusion.38
  33.3 0.1 fusion.40
  33.4 0.1 fusion.42
  33.5 78.2 %all-reduce.1 = bf16[16,1536]{1,0:T(8,128)(2,1)S(1)} all-reduce(f32[16,1536]{1,0:T(8,128)S(1)} %pad_maximum_fusion), channel_id=3, replica_groups=mesh['ep'=16,'tp'=2] {'ep'}, use_global_device_ids=true, to_apply=%region_1.0.clone | all-reduce | flops 24576 | bytes 147456
  111.7 0.7 dynamic-slice_convert_fusion
  112.4 1.2 multiply_add_fusion
  113.6 0.0 copy-start.1
  113.6 0.8 copy-done.1
  114.4 0.4 fusion.12
  114.8 0.6 multiply_reduce_fusion.3
  116.1 36.5 %all-gather.1 = bf16[32,1,512]{2,1,0:T(2,128)(2,1)S(1)} all-gather(bf16[1,1,512]{2,1,0:T(2,128)(2,1)S(1)} %reshape.496), channel_id=2, replica_groups=mesh['ep'=16,'tp'=2] {'ep','tp'}, dimensions={0}, use_global_device_ids=true | all-gather | bytes 33792 | tf_op jit(solution)/shard_map/all_gather | solution.py:120
  152.6 6.4 %fusion = f32[32,1,128]{2,1,0:T(1,128)S(1)} fusion(bf16[32,512,128]{2,0,1:T(8,128)(2,1)} %convolution_convert_fusion, bf16[32,1,512]{2,1,0:T(2,128)(2,1)S(1)} %all-gather.1), kind=kOutput, calls=%fused_computation.3 | convolution fusion | flops 4194304 | bytes 4243456 | tf_op jit(solution)/shard_map/msc,mcd->msd/dot_general | solution.py:128
  159.1 0.6 copy.73
  159.7 3.4 %all-to-all-start.4 = ((bf16[16,1,128]{2,1,0:T(2,128)(2,1)}), bf16[16,1,128]{2,1,0:T(2,128)(2,1)S(1)}, u32[]{:S(2)}, u32[]{:S(2)}) async-start(bf16[16,1,128]{2,1,0:T(2,128)(2,1)} %copy.73), calls=%async_computation.4 | async-start | bytes 16384 | tf_op jit(solution)/shard_map/all_to_all | solution.py:144
  163.2 0.8 gather_fusion
  163.9 0.6 reshape.471
  164.6 5.8 %all-to-all-done.4 = bf16[16,1,128]{2,1,0:T(2,128)(2,1)S(1)} async-done(((bf16[16,1,128]{2,1,0:T(2,128)(2,1)}), bf16[16,1,128]{2,1,0:T(2,128)(2,1)S(1)}, u32[]{:S(2)}, u32[]{:S(2)}) %all-to-all-start.4) | async-done | bytes 4128 | tf_op jit(solution)/shard_map/all_to_all | solution.py:144
  170.4 3.5 %all-to-all-start.2 = ((bf16[16,12,128]{2,1,0:T(8,128)(2,1)}), bf16[16,12,128]{2,1,0:T(8,128)(2,1)S(1)}, u32[]{:S(2)}, u32[]{:S(2)}) async-start(bf16[16,12,128]{2,1,0:T(8,128)(2,1)} %reshape.471), calls=%async_computation.2 | async-start | bytes 131072 | tf_op jit(solution)/shard_map/all_to_all | solution.py:143
  173.9 0.6 multiply_reduce_fusion.1
  175.3 0.2 fusion.64
  175.5 0.3 fusion.65
  175.8 1.5 fusion.66
  177.3 4.1 %all-to-all-done.2 = bf16[16,12,128]{2,1,0:T(8,128)(2,1)S(1)} async-done(((bf16[16,12,128]{2,1,0:T(8,128)(2,1)}), bf16[16,12,128]{2,1,0:T(8,128)(2,1)S(1)}, u32[]{:S(2)}, u32[]{:S(2)}) %all-to-all-start.2) | async-done | bytes 49184 | tf_op jit(solution)/shard_map/all_to_all | solution.py:143
  181.4 0.1 fusion.15
  181.5 0.1 fusion.18
  181.7 1.5 fusion.9
  183.2 2.0 fusion.2
  185.1 3.6 %all-reduce.2 = (bf16[1,12,2048]{2,1,0:T(8,128)(2,1)S(1)}, bf16[1,1,2048]{2,1,0:T(2,128)(2,1)S(1)}) all-reduce(bf16[1,12,2048]{2,1,0:T(8,128)(2,1)S(1)} %fusion.2, bf16[1,1,2048]{2,1,0:T(2,128)(2,1)S(1)} %convert_element_type.218), channel_id=1, replica_groups=mesh['ep'=16,'tp'=2] {'tp'}, use_global_device_ids=true, to_apply=%region_8.9 | all-reduce | flops 26624 | bytes 106496 | tf_op jit(solution)/shard_map/psum | solution.py:157
  188.7 2.1 copy.74
  190.8 3.8 %all-to-all-start.5 = ((bf16[1,1,2048]{1,0,2:T(2,128)(2,1)}), bf16[1,1,2048]{1,0,2:T(2,128)(2,1)S(1)}, u32[]{:S(2)}, u32[]{:S(2)}) async-start(bf16[1,1,2048]{1,0,2:T(2,128)(2,1)} %copy.74), calls=%async_computation.5 | async-start | bytes 2097152 | tf_op jit(solution)/shard_map/all_to_all | solution.py:164
  194.6 0.1 copy.72
  194.7 0.8 copy.69
  195.6 0.5 broadcast.257
  196.1 12.4 %reduce.11 = bf16[2048,12]{1,0:T(8,128)(2,1)} reduce(bf16[2048,1,12]{2,1,0:T(2,128)(2,1)S(1)} %bitcast.139, bf16[]{:T(256)} %broadcast.257), dimensions={1}, to_apply=%bitcast.122.reduce_sub_computation | reduce | bytes 98306
  208.4 2.4 reshape.519
  210.9 8.5 %all-to-all-done.5 = bf16[1,1,2048]{1,0,2:T(2,128)(2,1)S(1)} async-done(((bf16[1,1,2048]{1,0,2:T(2,128)(2,1)}), bf16[1,1,2048]{1,0,2:T(2,128)(2,1)S(1)}, u32[]{:S(2)}, u32[]{:S(2)}) %all-to-all-start.5) | async-done | bytes 4128 | tf_op jit(solution)/shard_map/all_to_all | solution.py:164
  219.3 6.8 %all-to-all-start.3 = ((bf16[16,2,768]{2,1,0:T(2,128)(2,1)}), bf16[16,2,768]{2,1,0:T(2,128)(2,1)S(1)}, u32[]{:S(2)}, u32[]{:S(2)}) async-start(bf16[16,2,768]{2,1,0:T(2,128)(2,1)} %reshape.519), calls=%async_computation.3 | async-start | bytes 98304 | tf_op jit(solution)/shard_map/all_to_all | solution.py:163
  226.1 15.2 %convert_reduce_fusion = f32[2048]{0:T(1024)S(1)} fusion(bf16[1,1,2048]{1,0,2:T(2,128)(2,1)S(1)} %all-to-all-done.5), kind=kLoop, calls=%fused_computation.17 | loop fusion | flops 2048 | bytes 12288 | tf_op jit(solution)/shard_map/convert_element_type | solution.py:168
  241.3 1.4 reshape.520
  242.8 0.6 copy.70
  243.4 0.7 gather_fusion.1
  244.1 0.1 multiply_reduce_fusion
  244.2 0.6 fusion.30
  (54 shorter events, 0.3 us)
Async XLA Ops:
  0.6 182.6 %copy-start = (bf16[1,256,2048]{2,1,0:T(8,128)(2,1)S(1)}, bf16[1,256,2048]{2,1,0:T(8,128)(2,1)}, u32[]{:S(2)}) copy-start(bf16[1,256,2048]{2,1,0:T(8,128)(2,1)} %param.38) | copy-start | bytes 3145732
  0.6 24.8 %copy-start.11 = (u32[32]{0:T(128)S(1)}, u32[32]{0:T(128)}, u32[]{:S(2)}) copy-start(u32[32]{0:T(128)} %constant.104) | copy-start | bytes 388
  0.7 32.3 %copy-start.4 = (bf16[128,512]{1,0:T(8,128)(2,1)S(1)}, bf16[128,512]{1,0:T(8,128)(2,1)}, u32[]{:S(2)}) copy-start(bf16[128,512]{1,0:T(8,128)(2,1)} %param.26) | copy-start | bytes 393220
  0.7 32.4 %copy-start.5 = (bf16[128,512]{1,0:T(8,128)(2,1)S(1)}, bf16[128,512]{1,0:T(8,128)(2,1)}, u32[]{:S(2)}) copy-start(bf16[128,512]{1,0:T(8,128)(2,1)} %param.25) | copy-start | bytes 393220
  0.7 32.6 %copy-start.6 = (bf16[128,256]{1,0:T(8,128)(2,1)S(1)}, bf16[128,256]{1,0:T(8,128)(2,1)}, u32[]{:S(2)}) copy-start(bf16[128,256]{1,0:T(8,128)(2,1)} %param.24) | copy-start | bytes 196612
  0.7 32.7 %copy-start.7 = (bf16[128,256]{1,0:T(8,128)(2,1)S(1)}, bf16[128,256]{1,0:T(8,128)(2,1)}, u32[]{:S(2)}) copy-start(bf16[128,256]{1,0:T(8,128)(2,1)} %param.23) | copy-start | bytes 196612
  4.1 21.9 %all-to-all-start.1 = ((bf16[1,16,128]{2,0,1:T(2,128)(2,1)}), bf16[1,16,128]{2,0,1:T(2,128)(2,1)S(1)}, u32[]{:S(2)}, u32[]{:S(2)}) async-start(bf16[1,16,128]{2,0,1:T(2,128)(2,1)} %convert_bitcast_fusion.3), calls=%async_computation.1 | async-start | bytes 16384 | tf_op jit(solution)/shard_map/all_to_all | solution.py:76
  13.5 102.5 %copy-start.10 = (f32[512]{0:T(512)S(1)}, f32[512]{0:T(512)}, u32[]{:S(2)}) copy-start(f32[512]{0:T(512)} %param.31) | copy-start | bytes 6148
  25.4 149.8 %copy-start.8 = (f32[2048]{0:T(1024)S(1)}, f32[2048]{0:T(1024)}, u32[]{:S(2)}) copy-start(f32[2048]{0:T(1024)} %param.33) | copy-start | bytes 24580
  25.4 149.8 %copy-start.2 = (bf16[2048,256]{1,0:T(8,128)(2,1)S(1)}, bf16[2048,256]{1,0:T(8,128)(2,1)}, u32[]{:S(2)}) copy-start(bf16[2048,256]{1,0:T(8,128)(2,1)} %param.39) | copy-start | bytes 3145732
  26.1 133.0 %all-to-all-start = ((bf16[1,16,128]{2,0,1:T(2,128)(2,1)}), bf16[1,16,128]{2,0,1:T(2,128)(2,1)S(1)}, u32[]{:S(2)}, u32[]{:S(2)}) async-start(bf16[1,16,128]{2,0,1:T(2,128)(2,1)} %bitcast), calls=%async_computation | async-start | bytes 16384 | tf_op jit(solution)/shard_map/all_to_all | solution.py:75
  33.5 142.0 %copy-start.3 = (bf16[2048,256]{1,0:T(8,128)(2,1)S(1)}, bf16[2048,256]{1,0:T(8,128)(2,1)}, u32[]{:S(2)}) copy-start(bf16[2048,256]{1,0:T(8,128)(2,1)} %param.40) | copy-start | bytes 3145732
  113.6 0.8 copy-start.1
  159.7 10.7 %all-to-all-start.4 = ((bf16[16,1,128]{2,1,0:T(2,128)(2,1)}), bf16[16,1,128]{2,1,0:T(2,128)(2,1)S(1)}, u32[]{:S(2)}, u32[]{:S(2)}) async-start(bf16[16,1,128]{2,1,0:T(2,128)(2,1)} %copy.73), calls=%async_computation.4 | async-start | bytes 16384 | tf_op jit(solution)/shard_map/all_to_all | solution.py:144
  170.4 11.0 %all-to-all-start.2 = ((bf16[16,12,128]{2,1,0:T(8,128)(2,1)}), bf16[16,12,128]{2,1,0:T(8,128)(2,1)S(1)}, u32[]{:S(2)}, u32[]{:S(2)}) async-start(bf16[16,12,128]{2,1,0:T(8,128)(2,1)} %reshape.471), calls=%async_computation.2 | async-start | bytes 131072 | tf_op jit(solution)/shard_map/all_to_all | solution.py:143
  175.8 18.9 %copy-start.9 = (f32[16,6]{0,1:T(8,128)S(1)}, f32[16,6]{0,1:T(8,128)}, u32[]{:S(2)}) copy-start(f32[16,6]{0,1:T(8,128)} %param.35) | copy-start | bytes 1156
  190.8 28.6 %all-to-all-start.5 = ((bf16[1,1,2048]{1,0,2:T(2,128)(2,1)}), bf16[1,1,2048]{1,0,2:T(2,128)(2,1)S(1)}, u32[]{:S(2)}, u32[]{:S(2)}) async-start(bf16[1,1,2048]{1,0,2:T(2,128)(2,1)} %copy.74), calls=%async_computation.5 | async-start | bytes 2097152 | tf_op jit(solution)/shard_map/all_to_all | solution.py:164
  219.3 22.0 %all-to-all-start.3 = ((bf16[16,2,768]{2,1,0:T(2,128)(2,1)}), bf16[16,2,768]{2,1,0:T(2,128)(2,1)S(1)}, u32[]{:S(2)}, u32[]{:S(2)}) async-start(bf16[16,2,768]{2,1,0:T(2,128)(2,1)} %reshape.519), calls=%async_computation.3 | async-start | bytes 98304 | tf_op jit(solution)/shard_map/all_to_all | solution.py:163
where the time goes:
time: 246 us; the launch traced here: 245 us
  blocking collectives  118 us (48%)
  other arithmetic  34.9 us (14%)
  starting transfers between devices  32.8 us (13%)
  local copies, waits for them, and re-layouts  19.3 us (8%)
  waiting for transfers between devices  18.4 us (7%)
  matrix products  18 us (7%)
  between operations  3.2 us (1%)
    unnamed x1, blocking collectives  78.2 us
    all_gather x1, blocking collectives, per_device(): shard_rows = lax.all_gather(mixed_heads, ('ep', 'tp'), axis=0, tiled=True)  36.5 us
    convert_element_type x1, other arithmetic, per_device(): back_shared.reshape(all_rows, -1).astype(jnp.float32)  15.2 us
    unnamed x1, other arithmetic  12.4 us
    all_to_all x1, waiting for transfers between devices, per_device(): lax.all_to_all(shared_out, 'ep', split_axis=2, concat_axis=0, tiled=True)  8.46 us
    all_to_all x1, starting transfers between devices, per_device(): lax.all_to_all(normed, 'ep', split_axis=1, concat_axis=0, tiled=True)  8.34 us
    all_to_all x1, starting transfers between devices, per_device(): lax.all_to_all(tokens, 'ep', split_axis=1, concat_axis=0, tiled=True)  6.91 us
    all_to_all x1, starting transfers between devices, per_device(): lax.all_to_all(routed_out, 'ep', split_axis=2, concat_axis=0, tiled=True)  6.75 us
  transfers between devices with their start and end apart: 6, of which 3 were waited for; matrix products, arithmetic and copies ran while one was open for 24% of the time, Pallas kernels for 0%

commit v1 on v0

--- a/solution.py
+++ b/solution.py
@@ -7,6 +7,13 @@
 DV = 512
 EPSILON = 1e-06
 DECAY_TEMPER = 16.0
+
+
+def swap_blocks(array, mesh_axis, split, join):
+    devices = lax.axis_size(mesh_axis)
+    blocks = jnp.stack(jnp.split(array, devices, axis=split), axis=0)
+    blocks = lax.all_to_all(blocks, mesh_axis, split_axis=0, concat_axis=0)
+    return jnp.concatenate(blocks, axis=join)
 
 
 def rms_scale(values):
@@ -161,7 +168,7 @@
     shared_out = shared_sum.astype(jnp.bfloat16)
     back_routed, back_shared = (
         lax.all_to_all(routed_out, "ep", split_axis=2, concat_axis=0, tiled=True),
-        lax.all_to_all(shared_out, "ep", split_axis=2, concat_axis=0, tiled=True),
+        swap_blocks(shared_out, "ep", 2, 0),
     )
     picked = back_routed.reshape(experts * capacity, -1)[flat_ids * capacity + position]
     weighted = picked.astype(jnp.float32).reshape(all_rows, top_count, -1) * route_weight[..., None]

time: 246 us -> 233 us (0.947)
  other arithmetic: 34.9 us -> 17.8 us
  local copies, waits for them, and re-layouts: 19.3 us -> 24.3 us
  starting transfers between devices: 32.8 us -> 29.7 us
    convert_element_type x1 -> x0, other arithmetic: 15.2 us -> none  [per_device(): back_shared.reshape(all_rows, -1).astype(jnp.float32)]
    all_to_all x1, waiting for transfers between devices: 0.01 us -> 6.89 us  [per_device(): lax.all_to_all(routed_out, 'ep', split_axis=2, concat_axis=0, tiled=True)]
    unnamed x35 -> x50, local copies, waits for them, and re-layouts: 6.68 us -> 13.2 us
    all_to_all x1, waiting for transfers between devices: 8.46 us -> 4.37 us  [swap_blocks(): blocks = lax.all_to_all(blocks, mesh_axis, split_axis=0, concat_axis=0)]
    all_to_all x1, starting transfers between devices: 6.75 us -> 4.01 us  [per_device(): lax.all_to_all(routed_out, 'ep', split_axis=2, concat_axis=0, tiled=True)]
  transfers between devices with their start and end apart: 6 -> 6, of which waited for: 3 -> 4; matrix products, arithmetic and copies ran while one was open for 24% -> 13% of each run, Pallas kernels for 0% -> 0%
where the time goes in v1:
time: 233 us
  blocking collectives  118 us (51%)
  starting transfers between devices  29.7 us (13%)
  local copies, waits for them, and re-layouts  24.3 us (10%)
  waiting for transfers between devices  20 us (9%)
  matrix products  19.3 us (8%)
  other arithmetic  17.8 us (8%)
  between operations  3.23 us (1%)
    unnamed x1, blocking collectives  78 us
    all_gather x1, blocking collectives, per_device(): shard_rows = lax.all_gather(mixed_heads, ('ep', 'tp'), axis=0, tiled=True)  36.5 us
    unnamed x50, local copies, waits for them, and re-layouts  13.2 us
    unnamed x1, other arithmetic  11.5 us
    all_to_all x1, starting transfers between devices, per_device(): lax.all_to_all(normed, 'ep', split_axis=1, concat_axis=0, tiled=True)  8.34 us
    all_to_all x1, starting transfers between devices, per_device(): lax.all_to_all(tokens, 'ep', split_axis=1, concat_axis=0, tiled=True)  6.91 us
    all_to_all x1, waiting for transfers between devices, per_device(): lax.all_to_all(routed_out, 'ep', split_axis=2, concat_axis=0, tiled=True)  6.89 us
    dot_general x1, matrix products, per_device(): jnp.einsum('msc,mcd->msd', shard_rows, chosen, preferred_element_type=jnp...  6.42 us
  transfers between devices with their start and end apart: 6, of which 4 were waited for; matrix products, arithmetic and copies ran while one was open for 13% of the time, Pallas kernels for 0%

profile of v1, /device:TPU:0, one launch (start us, length us, event | category | flops | bytes accessed | tf_op | source)
XLA Modules:
  0.0 232.6 jit_solution(17095565702015999689)
XLA Ops:
  0.7 1.4 multiply_reduce_fusion.2
  2.9 1.3 convert_bitcast_fusion.3
  4.2 8.3 %all-to-all-start.1 = ((bf16[1,16,128]{2,0,1:T(2,128)(2,1)}), bf16[1,16,128]{2,0,1:T(2,128)(2,1)S(1)}, u32[]{:S(2)}, u32[]{:S(2)}) async-start(bf16[1,16,128]{2,0,1:T(2,128)(2,1)} %convert_bitcast_fusion.3), calls=%async_computation.1 | async-start | bytes 16384 | tf_op jit(solution)/shard_map/all_to_all | solution.py:83
  12.5 0.8 copy.99
  13.6 0.1 reduce_window_sum.11
  13.7 0.2 select_reduce_fusion
  13.9 5.4 %scatter_fusion = s32[16,12]{1,0:T(8,128)S(1)} fusion(s32[16,12]{1,0:T(8,128)S(1)} %broadcast_in_dim.7, s32[96]{0:T(128)S(1)} %get-tuple-element.7, s32[96]{0:T(128)S(1)} %and_select_fusion), kind=kCustom, calls=%fused_computation.2 | custom fusion | bytes 1920 | tf_op jit(solution)/shard_map/scatter | solution.py:146
  19.5 1.1 fusion.11
  20.6 0.7 fusion.51
  21.3 4.2 %convolution_convert_fusion = bf16[32,512,128]{2,0,1:T(8,128)(2,1)} fusion(bf16[2,512,128]{2,1,0:T(8,128)(2,1)} %bitcast.204, s32[32]{0:T(128)S(1)} %and_select_fusion.1), kind=kOutput, calls=%fused_computation.5 | convolution fusion | flops 10485824 | bytes 4456576 | tf_op jit(solution)/shard_map/mt,tcd->mcd/dot_general | solution.py:132
  25.6 0.6 dynamic-slice
  26.2 6.9 %all-to-all-start = ((bf16[1,16,128]{2,0,1:T(2,128)(2,1)}), bf16[1,16,128]{2,0,1:T(2,128)(2,1)S(1)}, u32[]{:S(2)}, u32[]{:S(2)}) async-start(bf16[1,16,128]{2,0,1:T(2,128)(2,1)} %bitcast), calls=%async_computation | async-start | bytes 16384 | tf_op jit(solution)/shard_map/all_to_all | solution.py:82
  33.4 0.1 fusion.40
  33.5 0.1 fusion.42
  33.7 78.0 %all-reduce.1 = bf16[16,1536]{1,0:T(8,128)(2,1)S(1)} all-reduce(f32[16,1536]{1,0:T(8,128)S(1)} %pad_maximum_fusion), channel_id=3, replica_groups=mesh['ep'=16,'tp'=2] {'ep'}, use_global_device_ids=true, to_apply=%region_1.0.clone | all-reduce | flops 24576 | bytes 147456
  111.7 0.7 dynamic-slice_convert_fusion
  112.4 0.1 multiply_add_fusion
  112.6 0.4 fusion.12
  113.0 0.6 multiply_reduce_fusion.3
  114.3 36.5 %all-gather.1 = bf16[32,1,512]{2,1,0:T(2,128)(2,1)S(1)} all-gather(bf16[1,1,512]{2,1,0:T(2,128)(2,1)S(1)} %reshape.491), channel_id=2, replica_groups=mesh['ep'=16,'tp'=2] {'ep','tp'}, dimensions={0}, use_global_device_ids=true | all-gather | bytes 33792 | tf_op jit(solution)/shard_map/all_gather | solution.py:127
  150.8 6.4 %fusion = f32[32,1,128]{2,1,0:T(1,128)S(1)} fusion(bf16[32,512,128]{2,0,1:T(8,128)(2,1)} %convolution_convert_fusion, bf16[32,1,512]{2,1,0:T(2,128)(2,1)S(1)} %all-gather.1), kind=kOutput, calls=%fused_computation.3 | convolution fusion | flops 4194304 | bytes 4243456 | tf_op jit(solution)/shard_map/msc,mcd->msd/dot_general | solution.py:135
  157.3 0.6 copy.106
  157.9 3.4 %all-to-all-start.4 = ((bf16[16,1,128]{2,1,0:T(2,128)(2,1)}), bf16[16,1,128]{2,1,0:T(2,128)(2,1)S(1)}, u32[]{:S(2)}, u32[]{:S(2)}) async-start(bf16[16,1,128]{2,1,0:T(2,128)(2,1)} %copy.106), calls=%async_computation.4 | async-start | bytes 16384 | tf_op jit(solution)/shard_map/all_to_all | solution.py:151
  161.4 0.8 gather_fusion
  162.1 0.6 reshape.466
  162.8 5.8 %all-to-all-done.4 = bf16[16,1,128]{2,1,0:T(2,128)(2,1)S(1)} async-done(((bf16[16,1,128]{2,1,0:T(2,128)(2,1)}), bf16[16,1,128]{2,1,0:T(2,128)(2,1)S(1)}, u32[]{:S(2)}, u32[]{:S(2)}) %all-to-all-start.4) | async-done | bytes 4128 | tf_op jit(solution)/shard_map/all_to_all | solution.py:151
  168.6 3.5 %all-to-all-start.2 = ((bf16[16,12,128]{2,1,0:T(8,128)(2,1)}), bf16[16,12,128]{2,1,0:T(8,128)(2,1)S(1)}, u32[]{:S(2)}, u32[]{:S(2)}) async-start(bf16[16,12,128]{2,1,0:T(8,128)(2,1)} %reshape.466), calls=%async_computation.2 | async-start | bytes 131072 | tf_op jit(solution)/shard_map/all_to_all | solution.py:150
  172.1 0.6 multiply_reduce_fusion.1
  173.5 0.2 fusion.64
  173.7 1.5 fusion.65
  175.2 1.5 fusion.66
  176.7 2.9 %all-to-all-done.2 = bf16[16,12,128]{2,1,0:T(8,128)(2,1)S(1)} async-done(((bf16[16,12,128]{2,1,0:T(8,128)(2,1)}), bf16[16,12,128]{2,1,0:T(8,128)(2,1)S(1)}, u32[]{:S(2)}, u32[]{:S(2)}) %all-to-all-start.2) | async-done | bytes 49184 | tf_op jit(solution)/shard_map/all_to_all | solution.py:150
  179.6 0.1 fusion.15
  179.9 1.5 fusion.9
  181.4 2.0 fusion.2
  183.3 3.8 %all-reduce.2 = (bf16[1,12,2048]{2,1,0:T(8,128)(2,1)S(1)}, bf16[1,1,2048]{2,1,0:T(2,128)(2,1)S(1)}) all-reduce(bf16[1,12,2048]{2,1,0:T(8,128)(2,1)S(1)} %fusion.2, bf16[1,1,2048]{2,1,0:T(2,128)(2,1)S(1)} %convert_element_type.218), channel_id=1, replica_groups=mesh['ep'=16,'tp'=2] {'tp'}, use_global_device_ids=true, to_apply=%region_8.9 | all-reduce | flops 26624 | bytes 106496 | tf_op jit(solution)/shard_map/psum | solution.py:164
  187.1 0.6 constant_dynamic-update-slice_fusion.15
  187.7 0.5 constant_dynamic-update-slice_fusion.14
  188.2 0.5 constant_dynamic-update-slice_fusion.13
  188.7 0.5 constant_dynamic-update-slice_fusion.12
  189.3 0.5 constant_dynamic-update-slice_fusion.11
  189.8 0.6 constant_dynamic-update-slice_fusion.10
  190.3 0.6 constant_dynamic-update-slice_fusion.9
  190.9 0.5 constant_dynamic-update-slice_fusion.8
  191.5 0.5 constant_dynamic-update-slice_fusion.7
  192.0 0.6 constant_dynamic-update-slice_fusion.6
  192.5 0.6 constant_dynamic-update-slice_fusion.5
  193.1 0.5 constant_dynamic-update-slice_fusion.4
  193.7 0.6 constant_dynamic-update-slice_fusion.3
  194.3 0.5 constant_dynamic-update-slice_fusion.2
  194.8 0.5 constant_dynamic-update-slice_fusion.1
  195.3 0.8 copy.102
  196.1 0.5 broadcast.256
  196.6 11.5 %reduce.9 = bf16[2048,12]{1,0:T(8,128)(2,1)S(1)} reduce(bf16[2048,1,12]{2,1,0:T(2,128)(2,1)S(1)} %bitcast.200, bf16[]{:T(256)} %broadcast.256), dimensions={1}, to_apply=%bitcast.183.reduce_sub_computation | reduce | bytes 98306
  208.2 1.6 reshape.513
  209.7 4.0 %all-to-all-start.3 = ((bf16[16,2,768]{2,1,0:T(2,128)(2,1)}), bf16[16,2,768]{2,1,0:T(2,128)(2,1)S(1)}, u32[]{:S(2)}, u32[]{:S(2)}) async-start(bf16[16,2,768]{2,1,0:T(2,128)(2,1)} %reshape.513), calls=%async_computation.3 | async-start | bytes 98304 | tf_op jit(solution)/shard_map/all_to_all | solution.py:170
  213.7 0.6 constant_dynamic-update-slice_fusion
  214.3 6.9 %all-to-all-done.3 = bf16[16,2,768]{2,1,0:T(2,128)(2,1)S(1)} async-done(((bf16[16,2,768]{2,1,0:T(2,128)(2,1)}), bf16[16,2,768]{2,1,0:T(2,128)(2,1)S(1)}, u32[]{:S(2)}, u32[]{:S(2)}) %all-to-all-start.3) | async-done | bytes 49184 | tf_op jit(solution)/shard_map/all_to_all | solution.py:170
  221.2 3.5 %all-to-all-start.5 = ((bf16[16,1,1,128]{3,2,1,0:T(2,128)(2,1)}), bf16[16,1,1,128]{3,2,1,0:T(2,128)(2,1)S(1)}, u32[]{:S(2)}, u32[]{:S(2)}) async-start(bf16[16,1,1,128]{3,2,1,0:T(2,128)(2,1)} %constant_dynamic-update-slice_fusion), calls=%async_computation.5 | async-start | bytes 16384 | tf_op jit(solution)/shard_map/all_to_all | solution.py:15
  224.7 1.4 reshape.514
  226.1 0.6 copy.103
  226.8 0.7 gather_fusion.1
  227.6 4.4 %all-to-all-done.5 = bf16[16,1,1,128]{3,2,1,0:T(2,128)(2,1)S(1)} async-done(((bf16[16,1,1,128]{3,2,1,0:T(2,128)(2,1)}), bf16[16,1,1,128]{3,2,1,0:T(2,128)(2,1)S(1)}, u32[]{:S(2)}, u32[]{:S(2)}) %all-to-all-start.5) | async-done | bytes 4128 | tf_op jit(solution)/shard_map/all_to_all | solution.py:15
  232.0 0.6 fusion.30
  (68 shorter events, 1.2 us)
Async XLA Ops:
  0.6 180.7 %copy-start = (bf16[1,256,2048]{2,1,0:T(8,128)(2,1)S(1)}, bf16[1,256,2048]{2,1,0:T(8,128)(2,1)}, u32[]{:S(2)}) copy-start(bf16[1,256,2048]{2,1,0:T(8,128)(2,1)} %param.38) | copy-start | bytes 3145732
  0.6 25.0 %copy-start.11 = (u32[32]{0:T(128)S(1)}, u32[32]{0:T(128)}, u32[]{:S(2)}) copy-start(u32[32]{0:T(128)} %constant.104) | copy-start | bytes 388
  0.7 24.9 %copy-start.9 = (f32[16,6]{0,1:T(8,128)S(1)}, f32[16,6]{0,1:T(8,128)}, u32[]{:S(2)}) copy-start(f32[16,6]{0,1:T(8,128)} %param.35) | copy-start | bytes 1156
  0.7 32.5 %copy-start.4 = (bf16[128,512]{1,0:T(8,128)(2,1)S(1)}, bf16[128,512]{1,0:T(8,128)(2,1)}, u32[]{:S(2)}) copy-start(bf16[128,512]{1,0:T(8,128)(2,1)} %param.26) | copy-start | bytes 393220
  0.7 32.6 %copy-start.5 = (bf16[128,512]{1,0:T(8,128)(2,1)S(1)}, bf16[128,512]{1,0:T(8,128)(2,1)}, u32[]{:S(2)}) copy-start(bf16[128,512]{1,0:T(8,128)(2,1)} %param.25) | copy-start | bytes 393220
  0.7 32.7 %copy-start.6 = (bf16[128,256]{1,0:T(8,128)(2,1)S(1)}, bf16[128,256]{1,0:T(8,128)(2,1)}, u32[]{:S(2)}) copy-start(bf16[128,256]{1,0:T(8,128)(2,1)} %param.24) | copy-start | bytes 196612
  0.7 32.8 %copy-start.7 = (bf16[128,256]{1,0:T(8,128)(2,1)S(1)}, bf16[128,256]{1,0:T(8,128)(2,1)}, u32[]{:S(2)}) copy-start(bf16[128,256]{1,0:T(8,128)(2,1)} %param.23) | copy-start | bytes 196612
  0.7 111.7 %copy-start.3 = (f32[1,1,256,512]{3,2,1,0:T(8,128)S(1)}, f32[1,1,256,512]{3,2,1,0:T(8,128)}, u32[]{:S(2)}) copy-start(f32[1,1,256,512]{3,2,1,0:T(8,128)} %param.30) | copy-start | bytes 1572868
  4.2 22.0 %all-to-all-start.1 = ((bf16[1,16,128]{2,0,1:T(2,128)(2,1)}), bf16[1,16,128]{2,0,1:T(2,128)(2,1)S(1)}, u32[]{:S(2)}, u32[]{:S(2)}) async-start(bf16[1,16,128]{2,0,1:T(2,128)(2,1)} %convert_bitcast_fusion.3), calls=%async_computation.1 | async-start | bytes 16384 | tf_op jit(solution)/shard_map/all_to_all | solution.py:83
  13.6 100.7 %copy-start.10 = (f32[512]{0:T(512)S(1)}, f32[512]{0:T(512)}, u32[]{:S(2)}) copy-start(f32[512]{0:T(512)} %param.31) | copy-start | bytes 6148
  25.5 147.9 %copy-start.8 = (f32[2048]{0:T(1024)S(1)}, f32[2048]{0:T(1024)}, u32[]{:S(2)}) copy-start(f32[2048]{0:T(1024)} %param.33) | copy-start | bytes 24580
  25.5 148.0 %copy-start.2 = (bf16[2048,256]{1,0:T(8,128)(2,1)S(1)}, bf16[2048,256]{1,0:T(8,128)(2,1)}, u32[]{:S(2)}) copy-start(bf16[2048,256]{1,0:T(8,128)(2,1)} %param.39) | copy-start | bytes 3145732
  26.2 131.1 %all-to-all-start = ((bf16[1,16,128]{2,0,1:T(2,128)(2,1)}), bf16[1,16,128]{2,0,1:T(2,128)(2,1)S(1)}, u32[]{:S(2)}, u32[]{:S(2)}) async-start(bf16[1,16,128]{2,0,1:T(2,128)(2,1)} %bitcast), calls=%async_computation | async-start | bytes 16384 | tf_op jit(solution)/shard_map/all_to_all | solution.py:82
  112.6 64.1 %copy-start.1 = (f32[1,1,256,512]{3,2,1,0:T(8,128)}, f32[1,1,256,512]{3,2,1,0:T(8,128)S(1)}, u32[]{:S(2)}) copy-start(f32[1,1,256,512]{3,2,1,0:T(8,128)S(1)} %multiply_add_fusion) | copy-start | bytes 1572868
  157.9 10.7 %all-to-all-start.4 = ((bf16[16,1,128]{2,1,0:T(2,128)(2,1)}), bf16[16,1,128]{2,1,0:T(2,128)(2,1)S(1)}, u32[]{:S(2)}, u32[]{:S(2)}) async-start(bf16[16,1,128]{2,1,0:T(2,128)(2,1)} %copy.106), calls=%async_computation.4 | async-start | bytes 16384 | tf_op jit(solution)/shard_map/all_to_all | solution.py:151
  168.6 11.0 %all-to-all-start.2 = ((bf16[16,12,128]{2,1,0:T(8,128)(2,1)}), bf16[16,12,128]{2,1,0:T(8,128)(2,1)S(1)}, u32[]{:S(2)}, u32[]{:S(2)}) async-start(bf16[16,12,128]{2,1,0:T(8,128)(2,1)} %reshape.466), calls=%async_computation.2 | async-start | bytes 131072 | tf_op jit(solution)/shard_map/all_to_all | solution.py:150
  209.7 11.5 %all-to-all-start.3 = ((bf16[16,2,768]{2,1,0:T(2,128)(2,1)}), bf16[16,2,768]{2,1,0:T(2,128)(2,1)S(1)}, u32[]{:S(2)}, u32[]{:S(2)}) async-start(bf16[16,2,768]{2,1,0:T(2,128)(2,1)} %reshape.513), calls=%async_computation.3 | async-start | bytes 98304 | tf_op jit(solution)/shard_map/all_to_all | solution.py:170
  221.2 10.7 %all-to-all-start.5 = ((bf16[16,1,1,128]{3,2,1,0:T(2,128)(2,1)}), bf16[16,1,1,128]{3,2,1,0:T(2,128)(2,1)S(1)}, u32[]{:S(2)}, u32[]{:S(2)}) async-start(bf16[16,1,1,128]{3,2,1,0:T(2,128)(2,1)} %constant_dynamic-update-slice_fusion), calls=%async_computation.5 | async-start | bytes 16384 | tf_op jit(solution)/shard_map/all_to_all | solution.py:15
